TPU v7x, 256 devices: a whole 4x4x8 slice. The times are simulated.
256 devices in a mesh: sp: 64 (over z, x, core), tp: 4 (over y).
Axes of the slice: x: 4, y: 4, z: 8, core: 2. Of those that a mesh axis runs over, the one named last changes fastest.
Arguments:
- queries: bfloat16 [8192, 2048], P('sp', 'tp'), may hold values from -6 to 6
- key_rows: bfloat16 [8192, 2048], P('sp', 'tp'), may hold values from -6 to 6
- value_rows: bfloat16 [8192, 2048], P('sp', 'tp'), may hold values from -6 to 6
- gate_input: bfloat16 [8192, 2048], P('sp', 'tp'), may hold values from -6 to 6
- log_decay: float32 [8192, 16], P('sp', 'tp'), may hold values from -0.6 to 0, as said below
- head_gain: float32 [2048], P('tp'), may hold values from 0.1 to 1.9
- out_weight: bfloat16 [2048, 2048], P('tp'), may hold values from -0.125 to 0.125
- residual: bfloat16 [8192, 2048], P('sp'), may hold values from -6 to 6
- mlp_gain: float32 [2048], replicated, may hold values from 0.1 to 1.9
- gate_weight: bfloat16 [2048, 5632], P('sp', 'tp'), may hold values from -0.125 to 0.125
- up_weight: bfloat16 [2048, 5632], P('sp', 'tp'), may hold values from -0.125 to 0.125
- down_weight: bfloat16 [5632, 2048], P('tp', 'sp'), may hold values from -0.078125 to 0.078125
Outputs:
- layer_out: bfloat16 [8192, 2048], P(('sp', 'tp'))
Inputs may be any that keep to these rules, and one draw needn't show every extreme that they name: log_decay holds the logarithm of a decay factor of each head at each position.
All inputs are finite; a program needn't handle non-finite values.
Results may differ from a plain program's by a relative error of at most 0.017.
Values may be sent and summed in bfloat16 or wider, within the bound.
A program may use at most 128 MiB of HBM per device.

v0:
```python
import jax
import jax.numpy as jnp
from jax import lax
from jax.sharding import Mesh
from jax.sharding import PartitionSpec as P

BLOCK = 128
SP = ("sp_0", "sp_1", "sp_2")
SP_TP = ("sp_0", "sp_1", "sp_2", "tp")


EPS = 1e-06


def gather_turned(arrays, axis, dims):
    turned = [jnp.moveaxis(a, dim, 0) for a, dim in zip(arrays, dims)]
    widths = [t[0].size for t in turned]
    both = jnp.concatenate([t.reshape(-1, w) for t, w in zip(turned, widths)], axis=1)
    filled = lax.all_gather(both, axis, axis=0, tiled=True)
    blocks = jnp.split(filled, [sum(widths[:k]) for k in range(1, len(widths))], axis=1)
    return tuple(
        (
            jnp.moveaxis(b.reshape(-1, *t.shape[1:]), 0, dim)
            for b, t, dim in zip(blocks, turned, dims)
        )
    )


def nothing_yet(x, identity):
    return jax.tree.map(
        lambda part, zero: jnp.zeros_like(part) + jnp.asarray(zero, part.dtype), x, identity
    )


def carried_in(x, axes, combine, identity):
    before = start = nothing_yet(x, identity)
    total = x
    for axis in reversed(axes):
        length, index = (lax.axis_size(axis), lax.axis_index(axis))
        pieces = jax.tree.map(
            lambda part, kind: lax.all_gather(part.astype(kind), axis),
            total,
            (jnp.bfloat16, jnp.bfloat16),
        )
        inside, total = (start, start)
        for k in range(length):
            passed = k < index
            total = combine(
                total, jax.tree.map(lambda part, own: part[k].astype(own.dtype), pieces, x)
            )
            inside = jax.tree.map(lambda new, old: jnp.where(passed, new, old), total, inside)
        before = combine(inside, before)
    return before


def copy_for_each(x, axis):
    length = lax.axis_size(axis)
    return lax.all_to_all(jnp.broadcast_to(x[None], (length, *x.shape)), axis, 0, 0, tiled=True)


def over_copies(x, axis):
    return copy_for_each(x, axis).astype(jnp.float32).sum(axis=0)


def split_up(x, dim, length):
    dims = x.shape
    blocks = x.reshape(*dims[:dim], length, dims[dim] // length, *dims[dim + 1 :])
    return jnp.moveaxis(blocks, dim, 0)


def sum_at_owner(x, axis, dim):
    blocks = split_up(x, dim, lax.axis_size(axis))
    arrived = lax.all_to_all(blocks, axis, split_axis=0, concat_axis=0, tiled=True)
    return arrived.astype(jnp.float32).sum(axis=0)


def rotate(values_in, positions):
    half = values_in.shape[-1] // 2
    freq = 10000.0 ** (-jnp.linspace(0.0, 1.0, half, dtype=jnp.float32))
    angles = positions * freq
    angles = jnp.concatenate([angles, angles], axis=-1)
    first = values_in[..., :half]
    second = values_in[..., half:]
    turned = jnp.concatenate([-second, first], axis=-1)
    return values_in * jnp.cos(angles) + turned * jnp.sin(angles)


def row_norm(stream, gain):
    return stream * lax.rsqrt(jnp.mean(stream * stream, axis=-1, keepdims=True) + EPS) * gain


def join_states(earlier, later):
    return (earlier[0] * later[0], later[0][:, None, None] * earlier[1] + later[1])


def body(
    queries,
    key_rows,
    value_rows,
    gate_input,
    log_decay,
    head_gain,
    out_weight,
    residual,
    mlp_gain,
    gate_weight,
    up_weight,
    down_weight,
):
    tok_rows = queries.shape[0]
    heads_here = log_decay.shape[1]
    head_size = head_gain.shape[0] // heads_here
    quarter = tok_rows // lax.axis_size("tp")
    full_gate, full_up, full_down = gather_turned(
        (gate_weight, up_weight, down_weight), SP, (0, 0, 1)
    )
    offset = lax.axis_index(SP) * tok_rows
    positions = (offset + lax.iota(jnp.int32, tok_rows)).astype(jnp.float32)[:, None, None]
    q_rot = rotate(
        queries.reshape(tok_rows, heads_here, head_size).astype(jnp.float32), positions
    ).astype(jnp.bfloat16)
    k_rot = (
        rotate(key_rows.reshape(tok_rows, heads_here, head_size).astype(jnp.float32), positions)
        * head_size ** (-0.5)
    ).astype(jnp.bfloat16)
    blocks = tok_rows // BLOCK
    q_blocks = q_rot.reshape(blocks, BLOCK, heads_here, head_size)
    k_blocks = k_rot.reshape(blocks, BLOCK, heads_here, head_size)
    v_blocks = value_rows.reshape(blocks, BLOCK, heads_here, head_size)
    cumul = jnp.cumsum(log_decay.reshape(blocks, BLOCK, heads_here), axis=1)
    by_head = cumul.transpose(0, 2, 1)
    lower = jnp.tril(jnp.ones((BLOCK, BLOCK), dtype=bool))
    spread = by_head[:, :, :, None] - by_head[:, :, None, :]
    weight = jnp.where(lower, jnp.exp(jnp.where(lower, spread, 0.0)), 0.0)
    scores = jnp.einsum("nthd,nshd->nhts", q_blocks, k_blocks, preferred_element_type=jnp.float32)
    probs = (scores * weight).astype(jnp.bfloat16)
    inner = jnp.einsum("nhts,nshe->nthe", probs, v_blocks, preferred_element_type=jnp.float32)
    k_weighted = (
        k_blocks.astype(jnp.float32) * jnp.exp(cumul[:, -1:, :] - cumul)[..., None]
    ).astype(jnp.bfloat16)
    contrib = jnp.einsum(
        "nshd,nshe->nhde", k_weighted, v_blocks, preferred_element_type=jnp.float32
    )
    totals = jnp.exp(cumul[:, -1, :])

    def advance(carry, items):
        state, prefix = carry
        factor, update = items
        return ((state * factor[:, None, None] + update, prefix * factor), (state, prefix))

    start_state = jnp.zeros((heads_here, head_size, head_size), jnp.float32)
    start_prefix = jnp.ones((heads_here,), jnp.float32)
    (dev_state, dev_total), (local_before, prefixes) = lax.scan(
        advance, (start_state, start_prefix), (totals, contrib)
    )
    _, incoming = carried_in((dev_total, dev_state), SP, join_states, (start_prefix, start_state))
    before = local_before + prefixes[:, :, None, None] * incoming[None]
    cross = jnp.einsum(
        "nthd,nhde->nthe", q_blocks.astype(jnp.float32), before, precision=lax.Precision.HIGHEST
    )
    cross = cross * jnp.exp(cumul)[..., None]
    result = (inner + cross).reshape(tok_rows, heads_here, head_size)
    result = row_norm(result, head_gain.reshape(heads_here, head_size)).reshape(
        tok_rows, heads_here * head_size
    )
    retained = (result * jax.nn.silu(gate_input.astype(jnp.float32))).astype(jnp.bfloat16)
    partial_value = jnp.dot(retained, out_weight, preferred_element_type=jnp.float32)
    mixed = over_copies(partial_value.astype(jnp.bfloat16), "tp").astype(jnp.float32)
    middle = (residual.astype(jnp.float32) + mixed).astype(jnp.bfloat16)
    normed = row_norm(middle.astype(jnp.float32), mlp_gain).astype(jnp.bfloat16)
    rows_mid = lax.dynamic_slice_in_dim(middle, lax.axis_index("tp") * quarter, quarter, 0)
    gate = jnp.dot(normed, full_gate, preferred_element_type=jnp.float32)
    upvals = jnp.dot(normed, full_up, preferred_element_type=jnp.float32)
    hidden = (jax.nn.silu(gate) * upvals).astype(jnp.bfloat16)
    ffn = sum_at_owner(
        jnp.dot(hidden, full_down, preferred_element_type=jnp.float32).astype(jnp.bfloat16), "tp", 0
    )
    return (rows_mid.astype(jnp.float32) + ffn).astype(jnp.bfloat16)


def solution(mesh):
    finer = Mesh(mesh.devices.reshape(8, 4, 2, mesh.shape["tp"]), ("sp_0", "sp_1", "sp_2", "tp"))
    in_specs = (
        P(SP, "tp"),
        P(SP, "tp"),
        P(SP, "tp"),
        P(SP, "tp"),
        P(SP, "tp"),
        P("tp"),
        P("tp", None),
        P(SP, None),
        P(),
        P(SP, "tp"),
        P(SP, "tp"),
        P("tp", SP),
    )
    out_specs = P(SP_TP, None)
    return jax.shard_map(body, mesh=finer, in_specs=in_specs, out_specs=out_specs, check_vma=False)
```

profile of v0, /device:TPU:1, one launch (start us, length us, event | category | flops | bytes accessed | tf_op | source)
XLA Modules:
  0.0 215.4 jit_solution(10362698421659114462)
XLA Ops:
  6.6 0.9 copy.69
  7.8 4.7 %all-gather = bf16[2,1,4]{2,1,0:T(2,128)(2,1)S(1)} all-gather(bf16[1,1,4]{2,1,0:T(2,128)(2,1)S(1)} %get-tuple-element.38), channel_id=2, replica_groups=mesh['sp_0'=8,'sp_1'=4,'sp_2'=2,'tp'=4] {'sp_2'}, dimensions={0}, use_global_device_ids=true | all-gather | bytes 24 | tf_op jit(solution)/shard_map/all_gather | solution.py:41
  13.0 0.9 copy_bitcast_fusion
  13.9 0.9 copy_bitcast_fusion.1
  15.1 1.2 fusion.39
  16.3 1.2 fusion.20
  17.6 2.0 all-gather.1
  19.6 6.0 %all-gather.2 = bf16[4,1,4]{2,1,0:T(2,128)(2,1)S(1)} all-gather(bf16[1,1,4]{2,1,0:T(2,128)(2,1)S(1)} %multiply_convert_fusion.2), channel_id=1, replica_groups=mesh['sp_0'=8,'sp_1'=4,'sp_2'=2,'tp'=4] {'sp_1'}, dimensions={0}, use_global_device_ids=true | all-gather | bytes 40 | tf_op jit(solution)/shard_map/all_gather | solution.py:41
  25.7 11.4 %all_gather.31 = bf16[4,4,128,128]{3,2,1,0:T(8,128)(2,1)S(1)} all-gather(bf16[1,4,128,128]{3,2,1,0:T(8,128)(2,1)S(1)} %fusion.90), channel_id=1, replica_groups=mesh['sp_0'=8,'sp_1'=4,'sp_2'=2,'tp'=4] {'sp_1'}, dimensions={0}, use_global_device_ids=true | all-gather | bytes 655360 | tf_op jit(solution)/shard_map/all_gather | solution.py:41
  37.0 0.8 fusion.84
  38.0 0.7 pad_maximum_fusion
  38.7 14.3 %all-gather.3 = bf16[8,1,4]{2,1,0:T(2,128)(2,1)S(1)} all-gather(bf16[1,1,4]{2,1,0:T(2,128)(2,1)S(1)} %fusion.164), channel_id=1, replica_groups=mesh['sp_0'=8,'sp_1'=4,'sp_2'=2,'tp'=4] {'sp_0'}, dimensions={0}, use_global_device_ids=true | all-gather | bytes 72 | tf_op jit(solution)/shard_map/all_gather | solution.py:41
  53.1 2.0 convolution_bitcast_fusion.1
  55.1 20.8 %all-gather.7.cloned.1.call-done = bf16[8,4,128,128]{3,2,1,0:T(8,128)(2,1)} async-done(((bf16[1,4,128,128]{3,2,1,0:T(8,128)(2,1)}), bf16[8,4,128,128]{3,2,1,0:T(8,128)(2,1)}) %all-gather.7.cloned.1.call-update) | async-done | bytes 1048592 | tf_op jit(solution)/shard_map/all_gather | solution.py:41
  76.0 2.3 %multiply_reduce_fusion = (f32[128,4]{0,1:T(4,128)S(1)}, f32[1,128,4,128]{1,3,2,0:T(8,128)S(1)}) fusion(f32[1,128,4,128]{1,3,2,0:T(8,128)} %convolution_bitcast_fusion.1, f32[128,4]{0,1:T(4,128)S(1)} %get-tuple-element.49, bf16[128,4,128]{2,0,1:T(8,128)(2,1)S(1)} %get-tuple-element.36, bf16[8,4,128,128]{3,2,1,0:T(8,128)(2,1)} %all-gather.7.cloned.1.call-done, ...), kind=kOutput, calls=%fused_computation.63 | convolution fusion | flops 104660480 | bytes 2494734 | tf_op jit(solution)/shard_map/nthd,nhde->nthe/dot_general | solution.py:158
  78.8 0.5 convolution_convert_fusion
  79.6 24.2 %all_to_all.10 = bf16[4,128,2048]{2,1,0:T(8,128)(2,1)S(1)} all-to-all(bf16[4,128,2048]{2,1,0:T(8,128)(2,1)S(1)} %broadcast_in_dim.36), channel_id=1, replica_groups=mesh['sp_0'=8,'sp_1'=4,'sp_2'=2,'tp'=4] {'tp'}, dimensions={0} | all-to-all | bytes 4194304 | tf_op jit(solution)/shard_map/all_to_all | solution.py:58
  103.8 0.4 convert_reduce_fusion
  104.4 78.6 %all-gather.9.cloned.1.call-done = bf16[2048,4224]{1,0:T(8,128)(2,1)} async-done(((bf16[32,4224]{1,0:T(8,128)(2,1)}), bf16[2048,4224]{1,0:T(8,128)(2,1)}) %all-gather.9.cloned.1.call-update) | async-done | bytes 17301520 | tf_op jit(solution)/shard_map/all_gather | solution.py:19
  183.0 3.7 %fusion.4 = f32[128,1408]{1,0:T(8,128)S(1)} fusion(bf16[2048,4224]{1,0:T(8,128)(2,1)} %all-gather.9.cloned.1.call-done, bf16[128,2048]{1,0:T(8,128)(2,1)S(1)} %get-tuple-element.19, f32[2048]{0:T(1024)S(1)} %copy-done.6, f32[128]{0:T(128)S(1)} %add_rsqrt_fusion.1), kind=kOutput, calls=%fused_computation.4 | convolution fusion | flops 739246080 | bytes 7021056 | tf_op jit(solution)/shard_map/dot_general | solution.py:172
  186.7 8.0 %fusion.9 = bf16[128,2048]{1,0:T(8,128)(2,1)} fusion(bf16[2048,4224]{1,0:T(8,128)(2,1)} %all-gather.9.cloned.1.call-done, f32[128,1408]{1,0:T(8,128)S(1)} %fusion.4, bf16[128,2048]{1,0:T(8,128)(2,1)S(1)} %get-tuple-element.19, f32[2048]{0:T(1024)S(1)} %copy-done.6, f32[128]{0:T(128)S(1)} %add_rsqrt_fusion.1), kind=kOutput, calls=%fused_computation.8 | convolution fusion | flops 1478787072 | bytes 13312512 | tf_op jit(solution)/shard_map/dot_general | solution.py:176
  194.7 4.0 %all-to-all-start.1 = ((bf16[4,32,2048]{2,1,0:T(8,128)(2,1)}), bf16[4,32,2048]{2,1,0:T(8,128)(2,1)S(1)}, u32[]{:S(2)}, u32[]{:S(2)}) async-start(bf16[4,32,2048]{2,1,0:T(8,128)(2,1)} %bitcast.176), calls=%async_computation.1 | async-start | bytes 1048576 | tf_op jit(solution)/shard_map/all_to_all | solution.py:73
  198.7 9.0 %all-to-all-done.1 = bf16[4,32,2048]{2,1,0:T(8,128)(2,1)S(1)} async-done(((bf16[4,32,2048]{2,1,0:T(8,128)(2,1)}), bf16[4,32,2048]{2,1,0:T(8,128)(2,1)S(1)}, u32[]{:S(2)}, u32[]{:S(2)}) %all-to-all-start.1) | async-done | bytes 524320 | tf_op jit(solution)/shard_map/all_to_all | solution.py:73
  207.8 0.7 add_convert_fusion.1
  (49 shorter events, 2.4 us)
Async XLA Ops:
  6.5 72.2 %copy-start = (bf16[512,2048]{1,0:T(8,128)(2,1)S(1)}, bf16[512,2048]{1,0:T(8,128)(2,1)}, u32[]{:S(2)}) copy-start(bf16[512,2048]{1,0:T(8,128)(2,1)} %param.20) | copy-start | bytes 6291460
  6.5 31.4 %copy-start.2 = (bf16[1408,32]{0,1:T(8,128)(2,1)S(1)}, bf16[1408,32]{0,1:T(8,128)(2,1)}, u32[]{:S(2)}) copy-start(bf16[1408,32]{0,1:T(8,128)(2,1)} %param.25) | copy-start | bytes 270340
  6.5 31.4 %copy-start.4 = (bf16[32,1408]{1,0:T(8,128)(2,1)S(1)}, bf16[32,1408]{1,0:T(8,128)(2,1)}, u32[]{:S(2)}) copy-start(bf16[32,1408]{1,0:T(8,128)(2,1)} %param.23) | copy-start | bytes 270340
  6.5 31.4 %copy-start.3 = (bf16[32,1408]{1,0:T(8,128)(2,1)S(1)}, bf16[32,1408]{1,0:T(8,128)(2,1)}, u32[]{:S(2)}) copy-start(bf16[32,1408]{1,0:T(8,128)(2,1)} %param.24) | copy-start | bytes 270340
  6.5 69.4 %all-gather.7.cloned.1.call-start = ((), (), s32[]{:S(2)}) async-start(), calls=%async_computation.2 | async-start | bytes 1179648 | tf_op jit(solution)/shard_map/all_gather | solution.py:41
  15.1 63.7 %copy-start.7 = (f32[512]{0:T(512)S(1)}, f32[512]{0:T(512)}, u32[]{:S(2)}) copy-start(f32[512]{0:T(512)} %param.19) | copy-start | bytes 6148
  37.9 145.1 %all-gather.9.cloned.1.call-start = ((), (), s32[]{:S(2)}) async-start(), calls=%async_computation.3 | async-start | bytes 17571840 | tf_op jit(solution)/shard_map/all_gather | solution.py:19
  55.1 23.7 %copy-start.5 = (bf16[128,512]{1,0:T(8,128)(2,1)S(1)}, bf16[128,512]{1,0:T(8,128)(2,1)}, u32[]{:S(2)}) copy-start(bf16[128,512]{1,0:T(8,128)(2,1)} %param.17) | copy-start | bytes 393220
  79.3 24.9 %copy-start.1 = (bf16[128,2048]{1,0:T(8,128)(2,1)S(1)}, bf16[128,2048]{1,0:T(8,128)(2,1)}, u32[]{:S(2)}) copy-start(bf16[128,2048]{1,0:T(8,128)(2,1)} %param.21) | copy-start | bytes 1572868
  79.3 103.7 %copy-start.6 = (f32[2048]{0:T(1024)S(1)}, f32[2048]{0:T(1024)}, u32[]{:S(2)}) copy-start(f32[2048]{0:T(1024)} %param.22) | copy-start | bytes 24580
  194.7 13.0 %all-to-all-start.1 = ((bf16[4,32,2048]{2,1,0:T(8,128)(2,1)}), bf16[4,32,2048]{2,1,0:T(8,128)(2,1)S(1)}, u32[]{:S(2)}, u32[]{:S(2)}) async-start(bf16[4,32,2048]{2,1,0:T(8,128)(2,1)} %bitcast.176), calls=%async_computation.1 | async-start | bytes 1048576 | tf_op jit(solution)/shard_map/all_to_all | solution.py:73
Sparse Core Ops, SparseCore 0:
  38.0 37.9 all-gather.6
  78.7 104.2 all-gather.8
where the time goes:
time: 216 us; the launch traced here: 215 us
  waiting for transfers between devices  108 us (50%)
  blocking collectives  62.5 us (29%)
  matrix products  17.7 us (8%)
  between operations  13.6 us (6%)
  other arithmetic  7.15 us (3%)
  starting transfers between devices  4.07 us (2%)
    all_gather x1, waiting for transfers between devices, gather_turned(): filled = lax.all_gather(both, axis, axis=0, tiled=True)  78.6 us
    all_gather x5, blocking collectives, carried_in(): lax.all_gather(part.astype(kind), axis)  38.3 us
    all_to_all x1, blocking collectives, copy_for_each(): lax.all_to_all(jnp.broadcast_to(x[None], (length, *x.shape)), axis, 0, 0,...  24.2 us
    all_gather x1, waiting for transfers between devices, carried_in(): lax.all_gather(part.astype(kind), axis)  20.8 us
    all_to_all x1, waiting for transfers between devices, sum_at_owner(): lax.all_to_all(blocks, axis, split_axis=0, concat_axis=0, tiled=True)  9.03 us
    dot_general x1, matrix products, body(): jnp.dot(hidden, full_down, preferred_element_type=jnp.float32)  8.02 us
  transfers between devices with their start and end apart: 3, of which 3 were waited for; matrix products, arithmetic and copies ran while one was open for 3% of the time, Pallas kernels for 0%

commit v1 on v0

v1 whole, which is shorter than its diff:
```python
import heapq

import jax
import jax.numpy as jnp
from jax import lax
from jax.experimental import pallas as pl
from jax.experimental.pallas import tpu as pltpu
from jax.sharding import Mesh
from jax.sharding import PartitionSpec as P

BF = jnp.bfloat16
F32 = jnp.float32
MESH = pl.DeviceIdType.MESH
HIGH = lax.Precision.HIGHEST
EPS = 1e-06

NZ, NX, NC, NT = 8, 4, 2, 4
SP = ("z", "x", "c")
TOK = 128
HD = 128
HEADS = 4
D = 2048
FF = 1408
ROWS = 32
QT = TOK // NT
GATE, UP, DOWN = 0, 1, 2

PIECE_US = 1.95
HOP_US = 1.9


def forward_reach(a, dx):
    if a == UP:
        return 4 if dx % 2 == 0 else 3
    return 4 if a == GATE else 3


def onward(a, dz, dx):
    links = []
    reach = forward_reach(a, dx)
    if dz == 0:
        along_z = ["z+", "z-"]
    elif dz <= reach:
        along_z = ["z+"] if dz < reach else []
    else:
        along_z = ["z-"] if NZ - dz < NZ - 1 - reach else []
    plus = True if a == UP else dz % 2 == 0
    if dx == 0:
        along_x = ["x+", "x-"]
    elif dx == 1:
        along_x = ["x+"] if plus else []
    elif dx == 3:
        along_x = [] if plus else ["x-"]
    else:
        along_x = []
    if a == UP:
        links += along_z
        if dz == 0:
            links += along_x
    else:
        if dx == 0:
            links += along_z
        links += along_x
    return links


def arrives_as(link, key):
    a, dz, dx = key
    if link == "z+":
        return (a, (dz + 1) % NZ, dx)
    if link == "z-":
        return (a, (dz - 1) % NZ, dx)
    if link == "x+":
        return (a, dz, (dx + 1) % NX)
    return (a, dz, (dx - 1) % NX)


def exchange_plan():
    rank = {GATE: 0, UP: 0, DOWN: 1}
    pending = {l: [] for l in ("z+", "z-", "x+", "x-")}
    free = dict.fromkeys(pending, 0.0)
    arrivals = []
    ops = []
    count = 0

    def ready(now, key):
        nonlocal count
        for link in onward(*key):
            count += 1
            heapq.heappush(pending[link], (rank[key[0]], now, count, key))

    for a in (GATE, UP, DOWN):
        ready(0.0, (a, 0, 0))
    now = 0.0
    while True:
        for link, queue in pending.items():
            if queue and free[link] <= now:
                _, since, _, key = heapq.heappop(queue)
                free[link] = now + PIECE_US
                ops.append((max(since, now - PIECE_US), 1, "send", link, key))
                count += 1
                heapq.heappush(arrivals, (now + PIECE_US + HOP_US, count, arrives_as(link, key)))
        times = [t for l, t in free.items() if pending[l] and t > now]
        if arrivals:
            times.append(arrivals[0][0])
        if not times:
            break
        now = min(times)
        while arrivals and arrivals[0][0] <= now:
            _, _, key = heapq.heappop(arrivals)
            ops.append((now, 0, "recv", None, key))
            ready(now, key)
    ops.sort(key=lambda op: (op[0], op[1]))
    return ops


PLAN = exchange_plan()
SENT = {a: sum(1 for op in PLAN if op[2] == "send" and op[4][0] == a) for a in (GATE, UP, DOWN)}

T_CONTRIB, T_GROUP, T_ALONG, T_BACK, T_SUM1, T_GATHER = 2.5, 8.0, 14.0, 19.0, 30.0, 37.0


def head_cols(h):
    return slice(h * HD, (h + 1) * HD)


def split_log(total):
    hi = total.astype(BF).astype(F32)
    rest = total - hi
    mid = rest.astype(BF).astype(F32)
    low = rest - mid
    i = lax.broadcasted_iota(jnp.int32, (16, HD), 0)
    return jnp.where(i == 0, hi, jnp.where(i == 1, mid, low)).astype(BF)


def join_log(tile):
    t = tile.astype(F32)
    return t[0:1] + t[1:2] + t[2:3]


def silu(v):
    return v * (1.0 / (1.0 + jnp.exp(-v)))


def kernel(
    q_ref, k_ref, v_ref, gi_ref, ld_ref, cos_ref, sin_ref, hg_ref, ow_ref, res_ref, mg_ref,
    gw_ref, uw_ref, dw_ref,
    out_ref,
    w, ldp, qrot, inner, ret, stout, stin, pre, zout, zin, bout, bin_, po, rs1, nfull, mid,
    gacc, uacc, hid, fo, rs2,
    w_recv, w_send, d_recv, d_send,
    g_recv, g_send, z_recv, z_send, b_recv, b_send, r_recv, r_send, n_recv, n_send, f_recv, f_send,
):
    z, x, c, t = lax.axis_index("z"), lax.axis_index("x"), lax.axis_index("c"), lax.axis_index("tp")
    pos = x * NC + c

    def group_peer(r):
        p = lax.rem(pos + r, NX * NC)
        return p, (z, lax.div(p, NC), lax.rem(p, NC), t)

    def z_peer(r):
        return (lax.rem(z + r, NZ), x, c, t)

    def tp_peer(r):
        j = lax.rem(t + r, NT)
        return j, (z, x, c, j)

    neighbours = {
        "z+": (lax.rem(z + 1, NZ), x, c, t),
        "z-": (lax.rem(z + NZ - 1, NZ), x, c, t),
        "x+": (z, lax.rem(x + 1, NX), c, t),
        "x-": (z, lax.rem(x + NX - 1, NX), c, t),
    }
    partner = (z, x, 1 - c, t)

    barrier = pltpu.get_barrier_semaphore()
    for r in range(1, NX * NC):
        pl.semaphore_signal(barrier, inc=1, device_id=group_peer(r)[1], device_id_type=MESH)
    for r in range(1, NZ):
        pl.semaphore_signal(barrier, inc=1, device_id=z_peer(r), device_id_type=MESH)
    for r in range(1, NT):
        pl.semaphore_signal(barrier, inc=1, device_id=tp_peer(r)[1], device_id_type=MESH)
    pl.semaphore_wait(barrier, NX * NC - 1 + NZ - 1 + NT - 1)

    own = {GATE: gw_ref, UP: uw_ref, DOWN: dw_ref}

    def rows_of(dz, dx, core):
        sz = lax.rem(z + NZ - dz, NZ)
        sx = lax.rem(x + NX - dx, NX)
        return pl.ds(pl.multiple_of(((sz * NX + sx) * NC + core) * ROWS, ROWS), ROWS)

    def at_home(key):
        a, dz, dx = key
        return w.at[a, rows_of(dz, dx, c), :]

    def source(key):
        return own[key[0]] if key[1:] == (0, 0) else at_home(key)

    def hop(link, key):
        a, dz, dx = arrives_as(link, key)
        return pltpu.make_async_remote_copy(
            src_ref=source(key), dst_ref=at_home(key), send_sem=w_send.at[key[0]],
            recv_sem=w_recv.at[a, dz, dx], device_id=neighbours[link], device_id_type=MESH,
        )

    def across(key):
        a, dz, dx = key
        return pltpu.make_async_remote_copy(
            src_ref=source(key), dst_ref=at_home(key), send_sem=d_send.at[a, dz],
            recv_sem=d_recv.at[a, dz], device_id=partner, device_id_type=MESH,
        )

    cursor = [0]

    def step(op):
        _, _, kind, link, key = op
        if kind == "send":
            hop(link, key).start()
        else:
            a, dz, dx = key
            pltpu.make_async_remote_copy(
                src_ref=at_home(key), dst_ref=at_home(key), send_sem=w_send.at[a],
                recv_sem=w_recv.at[a, dz, dx], device_id=partner, device_id_type=MESH,
            ).wait_recv()
            across(key).start()

    def run_until(time):
        while cursor[0] < len(PLAN) and PLAN[cursor[0]][0] <= time:
            step(PLAN[cursor[0]])
            cursor[0] += 1

    def run_until_received(wanted):
        last = max(i for i, op in enumerate(PLAN) if op[2] == "recv" and wanted(op[4]))
        while cursor[0] <= last:
            step(PLAN[cursor[0]])
            cursor[0] += 1

    def wait_across(a, dz):
        whole = w.at[a, pl.ds(0, NX * ROWS), :]
        pltpu.make_async_remote_copy(
            src_ref=whole, dst_ref=whole, send_sem=d_send.at[a, dz],
            recv_sem=d_recv.at[a, dz], device_id=partner, device_id_type=MESH,
        ).wait_recv()

    run_until(0.0)
    for a in (GATE, UP, DOWN):
        across((a, 0, 0)).start()

    ldp[...] = jnp.zeros((TOK, HD), F32)
    ldp[:, 0:HEADS] = ld_ref[...]
    ti = lax.broadcasted_iota(jnp.int32, (TOK, TOK), 0)
    si = lax.broadcasted_iota(jnp.int32, (TOK, TOK), 1)
    lower = si <= ti
    cum = jnp.dot(lower.astype(F32), ldp[...], precision=HIGH, preferred_element_type=F32)
    cum_t = cum.T
    cosv, sinv = cos_ref[...], sin_ref[...]
    krots = []
    for h in range(HEADS):
        kf = k_ref[:, head_cols(h)].astype(F32)
        krot = ((kf * cosv + pltpu.roll(kf, HD // 2, 1) * sinv) * HD ** (-0.5)).astype(BF)
        krots.append(krot)
        col = cum[:, h : h + 1]
        last = cum[TOK - 1 : TOK, h : h + 1]
        kw = (krot.astype(F32) * jnp.exp(last - col)).astype(BF)
        contrib = jnp.dot(kw.T, v_ref[:, head_cols(h)], preferred_element_type=F32)
        logs = split_log(jnp.broadcast_to(last, (1, HD)))
        for half in range(2):
            stout[2 * h + half, 0:64, :] = contrib[64 * half : 64 * half + 64].astype(BF)
            stout[2 * h + half, 64:80, :] = logs
    for a in (GATE, UP, DOWN):
        w[a, rows_of(0, 0, c), :] = own[a][...]
    run_until(T_CONTRIB)

    def group_copy(r):
        p, peer = group_peer(r)
        return pltpu.make_async_remote_copy(
            src_ref=stout.at[p], dst_ref=stin.at[pos], send_sem=g_send.at[r],
            recv_sem=g_recv.at[r], device_id=peer, device_id_type=MESH,
        )

    for r in range(1, NX * NC):
        group_copy(r).start()
    stin[pos] = stout[pos]

    for h in range(HEADS):
        qf = q_ref[:, head_cols(h)].astype(F32)
        qr = (qf * cosv + pltpu.roll(qf, HD // 2, 1) * sinv).astype(BF)
        qrot[:, head_cols(h)] = qr
        spread = cum[:, h : h + 1] - cum_t[h : h + 1, :]
        weight = jnp.where(lower, jnp.exp(jnp.where(lower, spread, 0.0)), 0.0)
        scores = lax.dot_general(qr, krots[h], (((1,), (1,)), ((), ())), preferred_element_type=F32)
        probs = (scores * weight).astype(BF)
        inner[:, head_cols(h)] = jnp.dot(probs, v_ref[:, head_cols(h)], preferred_element_type=F32)
    run_until(T_GROUP)

    for r in range(1, NX * NC):
        group_copy(r).wait_recv()
    run = jnp.zeros((64, HD), F32)
    sofar = jnp.zeros((1, HD), F32)
    reach = []
    for p in range(NX * NC):
        pre[p] = run
        reach.append(sofar)
        log = join_log(stin[p, 64:80, :])
        run = run * jnp.exp(log) + stin[p, 0:64, :].astype(F32)
        sofar = sofar + log
    zout[0:64, :] = run.astype(BF)
    zout[64:80, :] = split_log(sofar)

    def z_copy(r):
        return pltpu.make_async_remote_copy(
            src_ref=zout, dst_ref=zin.at[z], send_sem=z_send.at[r],
            recv_sem=z_recv.at[r], device_id=z_peer(r), device_id_type=MESH,
        )

    for r in range(1, NZ):
        z_copy(r).start()
    zin[z] = zout[...]
    run_until(T_ALONG)
    for r in range(1, NZ):
        z_copy(r).wait_recv()
    came = jnp.zeros((64, HD), F32)
    for s in range(NZ):
        log = join_log(zin[s, 64:80, :])
        came = jnp.where(s < z, came * jnp.exp(log) + zin[s, 0:64, :].astype(F32), came)
    for p in range(NX * NC):
        bout[p] = (pre[p] + jnp.exp(reach[p]) * came).astype(BF)

    def back_copy(r):
        p, peer = group_peer(r)
        return pltpu.make_async_remote_copy(
            src_ref=bout.at[p], dst_ref=bin_.at[pos], send_sem=b_send.at[r],
            recv_sem=b_recv.at[r], device_id=peer, device_id_type=MESH,
        )

    for r in range(1, NX * NC):
        back_copy(r).start()
    bin_[pos] = bout[pos]
    run_until(T_BACK)
    for r in range(1, NX * NC):
        back_copy(r).wait_recv()

    for h in range(HEADS):
        before = bin_[2 * h : 2 * h + 2].reshape(HD, HD)
        cross = jnp.dot(qrot[:, head_cols(h)], before, preferred_element_type=F32)
        res = inner[:, head_cols(h)] + cross * jnp.exp(cum[:, h : h + 1])
        scale = lax.rsqrt(jnp.mean(res * res, axis=-1, keepdims=True) + EPS)
        gain = hg_ref[:, head_cols(h)]
        ret[:, head_cols(h)] = (
            res * scale * gain * silu(gi_ref[:, head_cols(h)].astype(F32))
        ).astype(BF)
    for n in range(0, D, 512):
        po[:, n : n + 512] = jnp.dot(
            ret[...], ow_ref[:, n : n + 512], preferred_element_type=F32
        ).astype(BF)

    mine = pl.ds(pl.multiple_of(t * QT, QT), QT)

    def sum_copy(r):
        j, peer = tp_peer(r)
        return pltpu.make_async_remote_copy(
            src_ref=po.at[pl.ds(pl.multiple_of(j * QT, QT), QT), :], dst_ref=rs1.at[r - 1],
            send_sem=r_send.at[r], recv_sem=r_recv.at[r], device_id=peer, device_id_type=MESH,
        )

    for r in (2, 1, 3):
        sum_copy(r).start()
    run_until(T_SUM1)
    for r in range(1, NT):
        sum_copy(r).wait_recv()
    mixed = po[mine, :].astype(F32)
    for r in range(NT - 1):
        mixed = mixed + rs1[r].astype(F32)
    middle = (res_ref[...].astype(F32) + mixed).astype(BF).astype(F32)
    mid[...] = middle
    scale = lax.rsqrt(jnp.mean(middle * middle, axis=-1, keepdims=True) + EPS)
    nfull[mine, :] = (middle * scale * mg_ref[...]).astype(BF)

    def norm_copy(r):
        return pltpu.make_async_remote_copy(
            src_ref=nfull.at[mine, :], dst_ref=nfull.at[mine, :],
            send_sem=n_send.at[r], recv_sem=n_recv.at[r], device_id=tp_peer(r)[1],
            device_id_type=MESH,
        )

    def norm_arrived(r):
        rows = nfull.at[pl.ds(pl.multiple_of(lax.rem(t + NT - r, NT) * QT, QT), QT), :]
        pltpu.make_async_remote_copy(
            src_ref=rows, dst_ref=rows, send_sem=n_send.at[r], recv_sem=n_recv.at[r],
            device_id=partner, device_id_type=MESH,
        ).wait_recv()

    for r in (2, 1, 3):
        norm_copy(r).start()
    run_until(T_GATHER)
    for r in range(1, NT):
        norm_arrived(r)

    run_until_received(lambda key: key[0] != DOWN)
    for a in (GATE, UP):
        for dz in range(NZ):
            wait_across(a, dz)
    clock = PLAN[cursor[0] - 1][0]
    for n in range(NZ):
        rows = slice(n * 256, (n + 1) * 256)
        for a, acc in ((GATE, gacc), (UP, uacc)):
            term = jnp.dot(nfull[:, rows], w[a, rows, :], preferred_element_type=F32)
            acc[...] = term if n == 0 else acc[...] + term
        clock += 0.6
        run_until(clock)
    hid[...] = (silu(gacc[...]) * uacc[...]).astype(BF)

    def ffn_copy(r, zc):
        j, peer = tp_peer(r)
        return pltpu.make_async_remote_copy(
            src_ref=fo.at[zc, pl.ds(pl.multiple_of(j * QT, QT), QT), :], dst_ref=rs2.at[r - 1, zc],
            send_sem=f_send.at[r], recv_sem=f_recv.at[r], device_id=peer, device_id_type=MESH,
        )

    last = {}
    for i, op in enumerate(PLAN):
        if op[2] == "recv" and op[4][0] == DOWN:
            last[op[4][1]] = i
    for dz in sorted(range(NZ), key=lambda k: last[k]):
        run_until_received(lambda key: key[0] == DOWN and key[1] == dz)
        wait_across(DOWN, dz)
        zc = lax.rem(z + NZ - dz, NZ)
        rows = pl.ds(pl.multiple_of(zc * 256, 256), 256)
        fo[zc] = lax.dot_general(
            hid[...], w[DOWN, rows, :], (((1,), (1,)), ((), ())), preferred_element_type=F32
        ).astype(BF)
        for r in (2, 1, 3):
            ffn_copy(r, zc).start()
    run_until(1e9)
    for r in range(1, NT):
        pltpu.make_async_remote_copy(
            src_ref=rs2.at[r - 1], dst_ref=rs2.at[r - 1], send_sem=f_send.at[r],
            recv_sem=f_recv.at[r], device_id=partner, device_id_type=MESH,
        ).wait_recv()
    for n in range(NZ):
        cols = slice(n * 256, (n + 1) * 256)
        total = fo[n, mine, :].astype(F32)
        for r in range(NT - 1):
            total = total + rs2[r, n].astype(F32)
        out_ref[:, cols] = (mid[:, cols] + total).astype(BF)

    for a in (GATE, UP, DOWN):
        sent = w.at[a, pl.ds(0, SENT[a] * ROWS), :]
        pltpu.make_async_remote_copy(
            src_ref=sent, dst_ref=sent, send_sem=w_send.at[a], recv_sem=w_recv.at[a, 0, 0],
            device_id=partner, device_id_type=MESH,
        ).wait_send()
        for dz in range(NZ):
            whole = w.at[a, pl.ds(0, NX * ROWS), :]
            pltpu.make_async_remote_copy(
                src_ref=whole, dst_ref=whole, send_sem=d_send.at[a, dz],
                recv_sem=d_recv.at[a, dz], device_id=partner, device_id_type=MESH,
            ).wait_send()
    for r in range(1, NX * NC):
        group_copy(r).wait_send()
        back_copy(r).wait_send()
    for r in range(1, NZ):
        z_copy(r).wait_send()
    for r in range(1, NT):
        sum_copy(r).wait_send()
        norm_copy(r).wait_send()
        pltpu.make_async_remote_copy(
            src_ref=rs2.at[r - 1], dst_ref=rs2.at[r - 1], send_sem=f_send.at[r],
            recv_sem=f_recv.at[r], device_id=partner, device_id_type=MESH,
        ).wait_send()


DMA = pltpu.SemaphoreType.DMA


def body(
    queries, key_rows, value_rows, gate_input, log_decay, head_gain, out_weight, residual,
    mlp_gain, gate_weight, up_weight, down_weight,
):
    half = HD // 2
    offset = lax.axis_index(SP) * TOK
    positions = (offset + lax.iota(jnp.int32, TOK)).astype(F32)[:, None]
    freq = 10000.0 ** (-jnp.linspace(0.0, 1.0, half, dtype=F32))
    angles = positions * freq
    cosv, sinv = jnp.cos(angles), jnp.sin(angles)
    cosv = jnp.concatenate([cosv, cosv], axis=-1)
    sinv = jnp.concatenate([-sinv, sinv], axis=-1)
    res = lax.dynamic_slice_in_dim(residual, lax.axis_index("tp") * QT, QT, 0)
    vmem = pl.BlockSpec(memory_space=pltpu.VMEM)
    V = pltpu.VMEM
    return pl.pallas_call(
        kernel,
        out_shape=jax.ShapeDtypeStruct((QT, D), BF),
        in_specs=[vmem] * 14,
        out_specs=vmem,
        scratch_shapes=[
            V((3, D, FF), BF),
            V((TOK, HD), F32),
            V((TOK, HEADS * HD), BF),
            V((TOK, HEADS * HD), F32),
            V((TOK, HEADS * HD), BF),
            V((8, 80, HD), BF),
            V((8, 80, HD), BF),
            V((8, 64, HD), F32),
            V((80, HD), BF),
            V((8, 80, HD), BF),
            V((8, 64, HD), BF),
            V((8, 64, HD), BF),
            V((TOK, D), BF),
            V((NT - 1, QT, D), BF),
            V((TOK, D), BF),
            V((QT, D), F32),
            V((TOK, FF), F32),
            V((TOK, FF), F32),
            V((TOK, FF), BF),
            V((NZ, TOK, 256), BF),
            V((NT - 1, NZ, QT, 256), BF),
            DMA((3, NZ, NX)),
            DMA((3,)),
            DMA((3, NZ)),
            DMA((3, NZ)),
            DMA((8,)), DMA((8,)), DMA((8,)), DMA((8,)), DMA((8,)), DMA((8,)),
            DMA((NT,)), DMA((NT,)), DMA((NT,)), DMA((NT,)), DMA((NT,)), DMA((NT,)),
        ],
        compiler_params=pltpu.CompilerParams(
            collective_id=0, has_side_effects=True, vmem_limit_bytes=56 * 1024 * 1024
        ),
    )(
        queries, key_rows, value_rows, gate_input, log_decay, cosv, sinv, head_gain[None, :],
        out_weight, res, mlp_gain[None, :], gate_weight, up_weight, down_weight.T,
    )


def solution(mesh):
    finer = Mesh(mesh.devices.reshape(NZ, NX, NC, NT), ("z", "x", "c", "tp"))
    in_specs = (
        P(SP, "tp"), P(SP, "tp"), P(SP, "tp"), P(SP, "tp"), P(SP, "tp"), P("tp"), P("tp", None),
        P(SP, None), P(), P(SP, "tp"), P(SP, "tp"), P("tp", SP),
    )
    out_specs = P(("z", "x", "c", "tp"), None)
    return jax.shard_map(body, mesh=finer, in_specs=in_specs, out_specs=out_specs, check_vma=False)
```

time: 216 us -> 93.7 us (0.43)
  waiting for transfers between devices: 108 us -> 0 us
  Pallas kernels: 0 us -> 88.7 us
  blocking collectives: 62.5 us -> 0 us
  matrix products: 17.7 us -> 0 us
  between operations: 13.6 us -> 0.02 us
  other arithmetic: 7.15 us -> 1.17 us
  starting transfers between devices: 4.07 us -> 0 us
    all_gather x2 -> x0, waiting for transfers between devices: 99.4 us -> none  [the longest x1 78.6 us: gather_turned(): filled = lax.all_gather(both, axis, axis=0, tiled=True)]
    pallas_call x0 -> x1, Pallas kernels: none -> 88.7 us  [body(): pl.pallas_call(kernel, out_shape=jax.ShapeDtypeStruct((QT, D), BF), in_sp...]
    all_gather x5 -> x0, blocking collectives: 38.3 us -> none  [carried_in(): lax.all_gather(part.astype(kind), axis)]
    all_to_all x1 -> x0, blocking collectives: 24.2 us -> none  [copy_for_each(): lax.all_to_all(jnp.broadcast_to(x[None], (length, *x.shape)), axis, 0, 0,...]
    dot_general x6 -> x0, matrix products: 17.7 us -> none  [the longest x1 8.02 us: body(): jnp.dot(hidden, full_down, preferred_element_type=jnp.float32)]
    all_to_all x1 -> x0, waiting for transfers between devices: 9.03 us -> none  [sum_at_owner(): lax.all_to_all(blocks, axis, split_axis=0, concat_axis=0, tiled=True)]
    convert_element_type x11 -> x1, other arithmetic: 4.71 us -> 0.01 us  [body(): positions = (offset + lax.iota(jnp.int32, TOK)).astype(F32)[:, None]]
    all_to_all x1 -> x0, starting transfers between devices: 3.99 us -> none  [sum_at_owner(): lax.all_to_all(blocks, axis, split_axis=0, concat_axis=0, tiled=True)]
  transfers between devices with their start and end apart: 3 -> 0, of which waited for: 3 -> 0; matrix products, arithmetic and copies ran while one was open for 3% -> 0% of each run, Pallas kernels for 0% -> 0%
where the time goes in v1:
time: 93.7 us; the launch traced here: 93.5 us
  Pallas kernels  88.7 us (95%)
  local copies, waits for them, and re-layouts  3.65 us (4%)
  other arithmetic  1.17 us (1%)
    pallas_call x1, Pallas kernels, body(): pl.pallas_call(kernel, out_shape=jax.ShapeDtypeStruct((QT, D), BF), in_sp...  88.7 us
    unnamed x4, local copies, waits for them, and re-layouts  2.98 us

profile of v1, /device:TPU:1, one launch (start us, length us, event | category | flops | bytes accessed | tf_op | source)
XLA Modules:
  0.0 93.5 jit_solution(5979429861900427534)
XLA Ops:
  0.0 0.0 copy-start
  0.0 0.1 fusion.1
  0.1 0.3 fusion
  0.4 0.8 pad_maximum_fusion
  1.2 0.0 copy-done
  1.2 0.7 constant_dynamic-slice_fusion.res_ref
  1.9 1.4 %copy.13.ld_ref = f32[128,4]{1,0:T(8,128)} copy(f32[128,4]{0,1:T(4,128)} %param.16) | data formatting | bytes 4096 | tf_op args[4]
  3.3 88.7 %shard_map.118 = bf16[32,2048]{1,0:T(8,128)(2,1)} custom-call(bf16[128,512]{1,0:T(8,128)(2,1)} %q_ref.1, bf16[128,512]{1,0:T(8,128)(2,1)} %k_ref.1, bf16[128,512]{1,0:T(8,128)(2,1)} %v_ref.1, bf16[128,512]{1,0:T(8,128)(2,1)} %gi_ref.1, f32[128,4]{1,0:T(8,128)} %copy.13.ld_ref, f32[128,128]{1,0:T(8,128)} %get-tuple-element.8.cos_ref, ...), custom_call_target="tpu_custom_call" | custom-call | tf_op jit(solution)/shard_map/pallas_call | solution.py:491
  92.0 1.6 %copy.15 = bf16[32,2048]{1,0:T(8,128)(2,1)} copy(bf16[32,2048]{1,0:T(8,128)(2,1)} %shard_map.118) | data formatting | bytes 262144
  (2 shorter events, 0.0 us)
Async XLA Ops:
  0.0 1.2 %copy-start = (bf16[128,2048]{1,0:T(8,128)(2,1)S(1)}, bf16[128,2048]{1,0:T(8,128)(2,1)}, u32[]{:S(2)}) copy-start(bf16[128,2048]{1,0:T(8,128)(2,1)} %param.19) | copy-start | bytes 1572868

commit v2 on v1

--- a/solution.py
+++ b/solution.py
@@ -2,6 +2,7 @@
 
 import jax
 import jax.numpy as jnp
+import numpy as np
 from jax import lax
 from jax.experimental import pallas as pl
 from jax.experimental.pallas import tpu as pltpu
@@ -25,69 +26,44 @@
 QT = TOK // NT
 GATE, UP, DOWN = 0, 1, 2
 
-PIECE_US = 1.95
-HOP_US = 1.9
-
-
-def forward_reach(a, dx):
-    if a == UP:
-        return 4 if dx % 2 == 0 else 3
-    return 4 if a == GATE else 3
-
-
-def onward(a, dz, dx):
-    links = []
-    reach = forward_reach(a, dx)
-    if dz == 0:
-        along_z = ["z+", "z-"]
-    elif dz <= reach:
-        along_z = ["z+"] if dz < reach else []
-    else:
-        along_z = ["z-"] if NZ - dz < NZ - 1 - reach else []
-    plus = True if a == UP else dz % 2 == 0
-    if dx == 0:
-        along_x = ["x+", "x-"]
-    elif dx == 1:
-        along_x = ["x+"] if plus else []
-    elif dx == 3:
-        along_x = [] if plus else ["x-"]
-    else:
-        along_x = []
-    if a == UP:
-        links += along_z
-        if dz == 0:
-            links += along_x
-    else:
-        if dx == 0:
-            links += along_z
-        links += along_x
-    return links
-
-
-def arrives_as(link, key):
+PIECE_US = 2.1
+HOP_US = 4.0
+LEAF_US = 2.0
+LEAD = 1.0
+LINKS = ("z+", "z-", "x+", "x-")
+CODES = (
+    16, 241, 134, 15, 144, 369, 6, 143, 272, 113, 138, 31, 32, 225, 150, 159, 160, 117, 10, 383,
+    230, 47, 48, 253, 122, 175, 164, 97, 154, 27, 176, 209, 234, 379, 64, 213, 126, 63, 180, 101,
+    54, 111, 40, 193, 238, 171, 188, 217, 70, 59, 76, 85, 186, 107, 288, 93, 198, 23, 204, 361,
+    222, 39, 72, 245, 90, 251, 200, 81, 294, 303, 304, 345, 374, 359, 264, 353, 278, 268, 365, 299,
+    310, 320, 329, 319, 350, 260, 285, 343, 282, 337, 312, 326, 335,
+)
+
+
+def sender_name(key, link):
     a, dz, dx = key
     if link == "z+":
+        return (a, (dz - 1) % NZ, dx)
+    if link == "z-":
         return (a, (dz + 1) % NZ, dx)
-    if link == "z-":
-        return (a, (dz - 1) % NZ, dx)
     if link == "x+":
-        return (a, dz, (dx + 1) % NX)
-    return (a, dz, (dx - 1) % NX)
+        return (a, dz, (dx - 1) % NX)
+    return (a, dz, (dx + 1) % NX)
 
 
 def exchange_plan():
-    rank = {GATE: 0, UP: 0, DOWN: 1}
-    pending = {l: [] for l in ("z+", "z-", "x+", "x-")}
-    free = dict.fromkeys(pending, 0.0)
-    arrivals = []
-    ops = []
-    count = 0
+    onward = {}
+    for turn, code in enumerate(CODES):
+        key, link = (code // 128, code // 16 % 8, code // 4 % 4), LINKS[code % 4]
+        onward.setdefault(sender_name(key, link), []).append((turn, link, key))
+    pending = {link: [] for link in LINKS}
+    free = dict.fromkeys(LINKS, 0.0)
+    arrivals, ops, since = [], [], {}
 
     def ready(now, key):
-        nonlocal count
-        for link in onward(*key):
-            count += 1
-            heapq.heappush(pending[link], (rank[key[0]], now, count, key))
+        for turn, link, there in onward.get(key, ()):
+            since[turn] = now
+            heapq.heappush(pending[link], (turn, there))
 
     for a in (GATE, UP, DOWN):
         ready(0.0, (a, 0, 0))
@@ -95,21 +71,26 @@
     while True:
         for link, queue in pending.items():
             if queue and free[link] <= now:
-                _, since, _, key = heapq.heappop(queue)
+                turn, key = heapq.heappop(queue)
                 free[link] = now + PIECE_US
-                ops.append((max(since, now - PIECE_US), 1, "send", link, key))
-                count += 1
-                heapq.heappush(arrivals, (now + PIECE_US + HOP_US, count, arrives_as(link, key)))
-        times = [t for l, t in free.items() if pending[l] and t > now]
-        if arrivals:
-            times.append(arrivals[0][0])
-        if not times:
+                ops.append((max(since[turn], now - LEAD * PIECE_US), 1, "send", link, key))
+                heapq.heappush(arrivals, (now + PIECE_US + HOP_US, key))
+        if not arrivals:
             break
-        now = min(times)
-        while arrivals and arrivals[0][0] <= now:
-            _, _, key = heapq.heappop(arrivals)
+        now = min([arrivals[0][0]] + [u for link, u in free.items() if pending[link] and u > now])
+        while arrivals and arrivals[0][0] <= now + 1e-9:
+            _, key = heapq.heappop(arrivals)
             ops.append((now, 0, "recv", None, key))
             ready(now, key)
+    due = {}
+    for time, _, kind, link, key in ops:
+        if kind == "send":
+            held = sender_name(key, link)
+            due[held] = min(time, due.get(held, time))
+    ops = [
+        (due.get(key, time + LEAF_US), order, kind, link, key) if kind == "recv" else (time, order, kind, link, key)
+        for time, order, kind, link, key in ops
+    ]
     ops.sort(key=lambda op: (op[0], op[1]))
     return ops
 
@@ -117,7 +98,7 @@
 PLAN = exchange_plan()
 SENT = {a: sum(1 for op in PLAN if op[2] == "send" and op[4][0] == a) for a in (GATE, UP, DOWN)}
 
-T_CONTRIB, T_GROUP, T_ALONG, T_BACK, T_SUM1, T_GATHER = 2.5, 8.0, 14.0, 19.0, 30.0, 37.0
+T_CONTRIB, T_GROUP, T_ALONG, T_BACK, T_SUM1, T_GATHER = 3.0, 8.0, 13.5, 18.0, 28.0, 36.0
 
 
 def head_cols(h):
@@ -143,9 +124,9 @@
 
 
 def kernel(
-    q_ref, k_ref, v_ref, gi_ref, ld_ref, cos_ref, sin_ref, hg_ref, ow_ref, res_ref, mg_ref,
-    gw_ref, uw_ref, dw_ref,
+    q_hbm, k_hbm, v_hbm, gi_hbm, ld_hbm, freq_hbm, hg_hbm, ow_hbm, res_hbm, mg_hbm, gw_hbm, uw_hbm, dw_hbm,
     out_ref,
+    q_ref, k_ref, v_ref, gi_ref, ld_ref, freq_ref, hg_ref, ow_ref, res_ref, mg_ref, gw_ref, uw_ref, dw_ref, in_sem,
     w, ldp, qrot, inner, ret, stout, stin, pre, zout, zin, bout, bin_, po, rs1, nfull, mid,
     gacc, uacc, hid, fo, rs2,
     w_recv, w_send, d_recv, d_send,
@@ -173,6 +154,23 @@
     }
     partner = (z, x, 1 - c, t)
 
+    mine = pl.ds(pl.multiple_of(t * QT, QT), QT)
+    inputs = {
+        "gw": (gw_hbm, gw_ref), "uw": (uw_hbm, uw_ref), "dw": (dw_hbm, dw_ref), "freq": (freq_hbm, freq_ref),
+        "ld": (ld_hbm, ld_ref), "k": (k_hbm, k_ref), "v": (v_hbm, v_ref), "q": (q_hbm, q_ref),
+        "gi": (gi_hbm, gi_ref), "hg": (hg_hbm, hg_ref), "ow": (ow_hbm, ow_ref),
+        "res": (res_hbm.at[mine, :], res_ref), "mg": (mg_hbm, mg_ref),
+    }
+    loads = {
+        name: pltpu.make_async_copy(src, dst, in_sem.at[i]) for i, (name, (src, dst)) in enumerate(inputs.items())
+    }
+    for load in loads.values():
+        load.start()
+
+    def loaded(*names):
+        for name in names:
+            loads[name].wait()
+
     barrier = pltpu.get_barrier_semaphore()
     for r in range(1, NX * NC):
         pl.semaphore_signal(barrier, inc=1, device_id=group_peer(r)[1], device_id_type=MESH)
@@ -180,6 +178,7 @@
         pl.semaphore_signal(barrier, inc=1, device_id=z_peer(r), device_id_type=MESH)
     for r in range(1, NT):
         pl.semaphore_signal(barrier, inc=1, device_id=tp_peer(r)[1], device_id_type=MESH)
+    loaded("gw", "uw", "dw")
     pl.semaphore_wait(barrier, NX * NC - 1 + NZ - 1 + NT - 1)
 
     own = {GATE: gw_ref, UP: uw_ref, DOWN: dw_ref}
@@ -197,9 +196,10 @@
         return own[key[0]] if key[1:] == (0, 0) else at_home(key)
 
     def hop(link, key):
-        a, dz, dx = arrives_as(link, key)
-        return pltpu.make_async_remote_copy(
-            src_ref=source(key), dst_ref=at_home(key), send_sem=w_send.at[key[0]],
+        a, dz, dx = key
+        held = sender_name(key, link)
+        return pltpu.make_async_remote_copy(
+            src_ref=source(held), dst_ref=at_home(held), send_sem=w_send.at[a],
             recv_sem=w_recv.at[a, dz, dx], device_id=neighbours[link], device_id_type=MESH,
         )
 
@@ -246,14 +246,20 @@
     for a in (GATE, UP, DOWN):
         across((a, 0, 0)).start()
 
+    loaded("freq")
+    row = lax.broadcasted_iota(jnp.int32, (TOK, HD), 0) + ((z * NX + x) * NC + c) * TOK
+    angles = row.astype(F32) * freq_ref[...]
+    cosv = jnp.cos(angles)
+    sinv = jnp.sin(angles)
+    sinv = jnp.where(lax.broadcasted_iota(jnp.int32, (TOK, HD), 1) < HD // 2, -sinv, sinv)
+    loaded("ld", "k", "v")
     ldp[...] = jnp.zeros((TOK, HD), F32)
-    ldp[:, 0:HEADS] = ld_ref[...]
+    ldp[0:HEADS, :] = ld_ref[...]
     ti = lax.broadcasted_iota(jnp.int32, (TOK, TOK), 0)
     si = lax.broadcasted_iota(jnp.int32, (TOK, TOK), 1)
     lower = si <= ti
-    cum = jnp.dot(lower.astype(F32), ldp[...], precision=HIGH, preferred_element_type=F32)
-    cum_t = cum.T
-    cosv, sinv = cos_ref[...], sin_ref[...]
+    cum_t = jnp.dot(ldp[...], (ti <= si).astype(F32), precision=HIGH, preferred_element_type=F32)
+    cum = cum_t.T
     krots = []
     for h in range(HEADS):
         kf = k_ref[:, head_cols(h)].astype(F32)
@@ -282,6 +288,7 @@
         group_copy(r).start()
     stin[pos] = stout[pos]
 
+    loaded("q")
     for h in range(HEADS):
         qf = q_ref[:, head_cols(h)].astype(F32)
         qr = (qf * cosv + pltpu.roll(qf, HD // 2, 1) * sinv).astype(BF)
@@ -340,6 +347,7 @@
     for r in range(1, NX * NC):
         back_copy(r).wait_recv()
 
+    loaded("gi", "hg", "ow", "res", "mg")
     for h in range(HEADS):
         before = bin_[2 * h : 2 * h + 2].reshape(HD, HD)
         cross = jnp.dot(qrot[:, head_cols(h)], before, preferred_element_type=F32)
@@ -353,8 +361,6 @@
         po[:, n : n + 512] = jnp.dot(
             ret[...], ow_ref[:, n : n + 512], preferred_element_type=F32
         ).astype(BF)
-
-    mine = pl.ds(pl.multiple_of(t * QT, QT), QT)
 
     def sum_copy(r):
         j, peer = tp_peer(r)
@@ -477,23 +483,19 @@
     queries, key_rows, value_rows, gate_input, log_decay, head_gain, out_weight, residual,
     mlp_gain, gate_weight, up_weight, down_weight,
 ):
-    half = HD // 2
-    offset = lax.axis_index(SP) * TOK
-    positions = (offset + lax.iota(jnp.int32, TOK)).astype(F32)[:, None]
-    freq = 10000.0 ** (-jnp.linspace(0.0, 1.0, half, dtype=F32))
-    angles = positions * freq
-    cosv, sinv = jnp.cos(angles), jnp.sin(angles)
-    cosv = jnp.concatenate([cosv, cosv], axis=-1)
-    sinv = jnp.concatenate([-sinv, sinv], axis=-1)
-    res = lax.dynamic_slice_in_dim(residual, lax.axis_index("tp") * QT, QT, 0)
+    freq = np.float32(10000.0 ** -np.linspace(0.0, 1.0, HD // 2))
+    freq = jnp.asarray(np.concatenate([freq, freq])[None, :])
     vmem = pl.BlockSpec(memory_space=pltpu.VMEM)
     V = pltpu.VMEM
     return pl.pallas_call(
         kernel,
         out_shape=jax.ShapeDtypeStruct((QT, D), BF),
-        in_specs=[vmem] * 14,
+        in_specs=[pl.BlockSpec(memory_space=pl.ANY)] * 13,
         out_specs=vmem,
         scratch_shapes=[
+            V((TOK, HEADS * HD), BF), V((TOK, HEADS * HD), BF), V((TOK, HEADS * HD), BF), V((TOK, HEADS * HD), BF),
+            V((HEADS, TOK), F32), V((1, HD), F32), V((1, HEADS * HD), F32), V((HEADS * HD, D), BF), V((QT, D), BF),
+            V((1, D), F32), V((ROWS, FF), BF), V((ROWS, FF), BF), V((ROWS, FF), BF), DMA((13,)),
             V((3, D, FF), BF),
             V((TOK, HD), F32),
             V((TOK, HEADS * HD), BF),
@@ -526,8 +528,8 @@
             collective_id=0, has_side_effects=True, vmem_limit_bytes=56 * 1024 * 1024
         ),
     )(
-        queries, key_rows, value_rows, gate_input, log_decay, cosv, sinv, head_gain[None, :],
-        out_weight, res, mlp_gain[None, :], gate_weight, up_weight, down_weight.T,
+        queries, key_rows, value_rows, gate_input, log_decay.T, freq, head_gain[None, :], out_weight, residual,
+        mlp_gain[None, :], gate_weight, up_weight, down_weight.T,
     )
 
 

time: 93.7 us -> 76.3 us (0.81)
  Pallas kernels: 88.7 us -> 74.6 us
  local copies, waits for them, and re-layouts: 3.65 us -> 1.57 us
  other arithmetic: 1.17 us -> 0 us
    pallas_call x1, Pallas kernels: 88.7 us -> 74.6 us  [body(): pl.pallas_call(kernel, out_shape=jax.ShapeDtypeStruct((QT, D), BF), in_sp...]
    unnamed x4 -> x1, local copies, waits for them, and re-layouts: 2.98 us -> 1.57 us
where the time goes in v2:
time: 76.3 us; the launch traced here: 76.2 us
  Pallas kernels  74.6 us (98%)
  local copies, waits for them, and re-layouts  1.57 us (2%)
    pallas_call x1, Pallas kernels, body(): pl.pallas_call(kernel, out_shape=jax.ShapeDtypeStruct((QT, D), BF), in_sp...  74.6 us
    unnamed x1, local copies, waits for them, and re-layouts  1.57 us

profile of v2, /device:TPU:1, one launch (start us, length us, event | category | flops | bytes accessed | tf_op | source)
XLA Modules:
  0.0 76.2 jit_solution(2032420256767844840)
XLA Ops:
  0.0 74.6 %shard_map.127 = bf16[32,2048]{1,0:T(8,128)(2,1)} custom-call(bf16[128,512]{1,0:T(8,128)(2,1)} %q_hbm.1, bf16[128,512]{1,0:T(8,128)(2,1)} %k_hbm.1, bf16[128,512]{1,0:T(8,128)(2,1)} %v_hbm.1, bf16[128,512]{1,0:T(8,128)(2,1)} %gi_hbm.1, f32[4,128]{1,0:T(4,128)} %bitcast.6, f32[1,128]{1,0:T(1,128)} %constant.2.clone.freq_hbm, f32[1,512]{1,0:T(1,128)} %bitcast.7, ...), custom_call_target="tpu_custom_call" | custom-call | tf_op jit(solution)/shard_map/pallas_call | solution.py:490
  74.7 1.6 %copy.15 = bf16[32,2048]{1,0:T(8,128)(2,1)} copy(bf16[32,2048]{1,0:T(8,128)(2,1)} %shard_map.127) | data formatting | bytes 262144

commit v3 on v2

--- a/solution.py
+++ b/solution.py
@@ -28,15 +28,15 @@
 
 PIECE_US = 2.1
 HOP_US = 4.0
-LEAF_US = 2.0
+LEAF_US = 0.5
 LEAD = 1.0
 LINKS = ("z+", "z-", "x+", "x-")
 CODES = (
-    16, 241, 134, 15, 144, 369, 6, 143, 272, 113, 138, 31, 32, 225, 150, 159, 160, 117, 10, 383,
-    230, 47, 48, 253, 122, 175, 164, 97, 154, 27, 176, 209, 234, 379, 64, 213, 126, 63, 180, 101,
-    54, 111, 40, 193, 238, 171, 188, 217, 70, 59, 76, 85, 186, 107, 288, 93, 198, 23, 204, 361,
-    222, 39, 72, 245, 90, 251, 200, 81, 294, 303, 304, 345, 374, 359, 264, 353, 278, 268, 365, 299,
-    310, 320, 329, 319, 350, 260, 285, 343, 282, 337, 312, 326, 335,
+    16, 241, 6, 143, 272, 113, 134, 271, 144, 369, 10, 31, 32, 225, 118, 127, 156, 97, 374, 255,
+    160, 245, 14, 239, 48, 209, 38, 111, 172, 81, 378, 27, 284, 101, 166, 47, 20, 93, 214, 63,
+    148, 65, 122, 171, 176, 193, 106, 235, 300, 77, 218, 59, 228, 197, 70, 251, 40, 85, 154, 191,
+    316, 89, 290, 283, 72, 357, 202, 383, 180, 53, 222, 187, 204, 137, 306, 279, 332, 341, 362, 355,
+    296, 365, 294, 315, 260, 265, 310, 331, 320, 325, 346, 339, 349,
 )
 
 
@@ -98,7 +98,7 @@
 PLAN = exchange_plan()
 SENT = {a: sum(1 for op in PLAN if op[2] == "send" and op[4][0] == a) for a in (GATE, UP, DOWN)}
 
-T_CONTRIB, T_GROUP, T_ALONG, T_BACK, T_SUM1, T_GATHER = 3.0, 8.0, 13.5, 18.0, 28.0, 36.0
+T_CONTRIB, T_GROUP, T_ALONG, T_BACK, T_SUM1, T_GATHER = 3.0, 10.0, 16.5, 22.5, 32.5, 41.0
 
 
 def head_cols(h):
@@ -127,7 +127,7 @@
     q_hbm, k_hbm, v_hbm, gi_hbm, ld_hbm, freq_hbm, hg_hbm, ow_hbm, res_hbm, mg_hbm, gw_hbm, uw_hbm, dw_hbm,
     out_ref,
     q_ref, k_ref, v_ref, gi_ref, ld_ref, freq_ref, hg_ref, ow_ref, res_ref, mg_ref, gw_ref, uw_ref, dw_ref, in_sem,
-    w, ldp, qrot, inner, ret, stout, stin, pre, zout, zin, bout, bin_, po, rs1, nfull, mid,
+    w, ldp, qrot, inner, ret, stout, stin, pre, came_ref, zout, zin, bout, bin_, po, rs1, nfull, mid,
     gacc, uacc, hid, fo, rs2,
     w_recv, w_send, d_recv, d_send,
     g_recv, g_send, z_recv, z_send, b_recv, b_send, r_recv, r_send, n_recv, n_send, f_recv, f_send,
@@ -321,15 +321,21 @@
         )
 
     for r in range(1, NZ):
-        z_copy(r).start()
-    zin[z] = zout[...]
+        @pl.when(z + r < NZ)
+        def _():
+            z_copy(r).start()
     run_until(T_ALONG)
     for r in range(1, NZ):
-        z_copy(r).wait_recv()
-    came = jnp.zeros((64, HD), F32)
-    for s in range(NZ):
-        log = join_log(zin[s, 64:80, :])
-        came = jnp.where(s < z, came * jnp.exp(log) + zin[s, 0:64, :].astype(F32), came)
+        @pl.when(z >= r)
+        def _():
+            z_copy(r).wait_recv()
+    came_ref[...] = jnp.zeros((64, HD), F32)
+    for s in range(NZ - 1):
+        @pl.when(s < z)
+        def _():
+            decay = jnp.exp(join_log(zin[s, 64:80, :]))
+            came_ref[...] = came_ref[...] * decay + zin[s, 0:64, :].astype(F32)
+    came = came_ref[...]
     for p in range(NX * NC):
         bout[p] = (pre[p] + jnp.exp(reach[p]) * came).astype(BF)
 
@@ -466,7 +472,9 @@
         group_copy(r).wait_send()
         back_copy(r).wait_send()
     for r in range(1, NZ):
-        z_copy(r).wait_send()
+        @pl.when(z + r < NZ)
+        def _():
+            z_copy(r).wait_send()
     for r in range(1, NT):
         sum_copy(r).wait_send()
         norm_copy(r).wait_send()
@@ -489,7 +497,7 @@
     V = pltpu.VMEM
     return pl.pallas_call(
         kernel,
-        out_shape=jax.ShapeDtypeStruct((QT, D), BF),
+        out_shape=pltpu.VMEM((QT, D), BF),
         in_specs=[pl.BlockSpec(memory_space=pl.ANY)] * 13,
         out_specs=vmem,
         scratch_shapes=[
@@ -504,6 +512,7 @@
             V((8, 80, HD), BF),
             V((8, 80, HD), BF),
             V((8, 64, HD), F32),
+            V((64, HD), F32),
             V((80, HD), BF),
             V((8, 80, HD), BF),
             V((8, 64, HD), BF),

time: 76.3 us -> 73 us (0.957)
  Pallas kernels: 74.6 us -> 72.3 us
  local copies, waits for them, and re-layouts: 1.57 us -> 0.66 us
    pallas_call x1, Pallas kernels: 74.6 us -> 72.3 us  [body(): pl.pallas_call(kernel, out_shape=pltpu.VMEM((QT, D), BF), in_specs=[pl.Bl...]
    unnamed x1, local copies, waits for them, and re-layouts: 1.57 us -> 0.66 us
where the time goes in v3:
time: 73 us; the launch traced here: 72.9 us
  Pallas kernels  72.3 us (99%)
    pallas_call x1, Pallas kernels, body(): pl.pallas_call(kernel, out_shape=pltpu.VMEM((QT, D), BF), in_specs=[pl.Bl...  72.3 us

profile of v3, /device:TPU:1, one launch (start us, length us, event | category | flops | bytes accessed | tf_op | source)
XLA Modules:
  0.0 72.9 jit_solution(7376470207093449875)
XLA Ops:
  0.0 72.3 %shard_map.127 = bf16[32,2048]{1,0:T(8,128)(2,1)S(1)} custom-call(bf16[128,512]{1,0:T(8,128)(2,1)} %q_hbm.1, bf16[128,512]{1,0:T(8,128)(2,1)} %k_hbm.1, bf16[128,512]{1,0:T(8,128)(2,1)} %v_hbm.1, bf16[128,512]{1,0:T(8,128)(2,1)} %gi_hbm.1, f32[4,128]{1,0:T(4,128)} %bitcast.6, f32[1,128]{1,0:T(1,128)} %constant.2.clone.freq_hbm, f32[1,512]{1,0:T(1,128)} %bitcast.7, ...), custom_call_target="tpu_custom_call" | custom-call | tf_op jit(solution)/shard_map/pallas_call | solution.py:498
  72.3 0.7 copy.15

commit v4 on v3

--- a/solution.py
+++ b/solution.py
@@ -32,11 +32,11 @@
 LEAD = 1.0
 LINKS = ("z+", "z-", "x+", "x-")
 CODES = (
-    16, 241, 6, 143, 272, 113, 134, 271, 144, 369, 10, 31, 32, 225, 118, 127, 156, 97, 374, 255,
-    160, 245, 14, 239, 48, 209, 38, 111, 172, 81, 378, 27, 284, 101, 166, 47, 20, 93, 214, 63,
-    148, 65, 122, 171, 176, 193, 106, 235, 300, 77, 218, 59, 228, 197, 70, 251, 40, 85, 154, 191,
-    316, 89, 290, 283, 72, 357, 202, 383, 180, 53, 222, 187, 204, 137, 306, 279, 332, 341, 362, 355,
-    296, 365, 294, 315, 260, 265, 310, 331, 320, 325, 346, 339, 349,
+    16, 241, 6, 271, 144, 113, 134, 15, 272, 225, 246, 267, 32, 97, 118, 127, 160, 22, 11, 377,
+    280, 230, 239, 101, 48, 166, 175, 81, 36, 250, 31, 213, 252, 382, 279, 85, 188, 54, 63, 209,
+    136, 106, 95, 233, 140, 370, 171, 365, 204, 178, 27, 45, 68, 218, 223, 77, 64, 374, 59, 153,
+    180, 194, 203, 109, 292, 90, 75, 349, 120, 158, 151, 357, 284, 186, 199, 41, 308, 338, 347, 333,
+    260, 362, 355, 341, 300, 298, 291, 324, 317, 322, 331, 314, 307,
 )
 
 
@@ -98,7 +98,7 @@
 PLAN = exchange_plan()
 SENT = {a: sum(1 for op in PLAN if op[2] == "send" and op[4][0] == a) for a in (GATE, UP, DOWN)}
 
-T_CONTRIB, T_GROUP, T_ALONG, T_BACK, T_SUM1, T_GATHER = 3.0, 10.0, 16.5, 22.5, 32.5, 41.0
+T_CONTRIB, T_GROUP, T_ALONG, T_BACK, T_SUM1, T_GATHER = 3.0, 11.0, 20.0, 28.0, 37.5, 46.0
 
 
 def head_cols(h):

time: 73 us -> 72.1 us (0.988)
  Pallas kernels: 72.3 us -> 71.4 us
    pallas_call x1, Pallas kernels: 72.3 us -> 71.4 us  [body(): pl.pallas_call(kernel, out_shape=pltpu.VMEM((QT, D), BF), in_specs=[pl.Bl...]
where the time goes in v4:
time: 72.1 us; the launch traced here: 72 us
  Pallas kernels  71.4 us (99%)
    pallas_call x1, Pallas kernels, body(): pl.pallas_call(kernel, out_shape=pltpu.VMEM((QT, D), BF), in_specs=[pl.Bl...  71.4 us

profile of v4, /device:TPU:1, one launch (start us, length us, event | category | flops | bytes accessed | tf_op | source)
XLA Modules:
  0.0 72.0 jit_solution(9399306322781603740)
XLA Ops:
  0.0 71.4 %shard_map.127 = bf16[32,2048]{1,0:T(8,128)(2,1)S(1)} custom-call(bf16[128,512]{1,0:T(8,128)(2,1)} %q_hbm.1, bf16[128,512]{1,0:T(8,128)(2,1)} %k_hbm.1, bf16[128,512]{1,0:T(8,128)(2,1)} %v_hbm.1, bf16[128,512]{1,0:T(8,128)(2,1)} %gi_hbm.1, f32[4,128]{1,0:T(4,128)} %bitcast.6, f32[1,128]{1,0:T(1,128)} %constant.2.clone.freq_hbm, f32[1,512]{1,0:T(1,128)} %bitcast.7, ...), custom_call_target="tpu_custom_call" | custom-call | tf_op jit(solution)/shard_map/pallas_call | solution.py:498
  71.4 0.7 copy.15
